TPU v7x, 32 devices: a whole 2x2x4 slice. The times are simulated.
32 devices in a mesh: sp: 8 (over z, x), tp: 4 (over y, core).
Axes of the slice: x: 2, y: 2, z: 4, core: 2. Of those that a mesh axis runs over, the one named last changes fastest.
Arguments:
- queries: bfloat16 [4096, 1024], P('sp', 'tp'), may hold values from -5.5 to 5.5
- key_vectors: bfloat16 [4096, 1024], P('sp', 'tp'), may hold values from -5.5 to 5.5
- latents: bfloat16 [4096, 2048], P('sp', 'tp'), may hold values from -6 to 6
- w_value: bfloat16 [2048, 1024], P(None, 'tp'), may hold values from -0.125 to 0.125
- log_sums: float32 [4096, 16], P('sp', 'tp'), as said below
- out_pair: bfloat16 [4096, 2048], P('sp', 'tp'), may hold values from -6 to 6
- cotangent: bfloat16 [4096, 1024], P('sp', 'tp'), may hold values from -6 to 6
- lambdas: float32 [8], P('tp'), may hold values from 0.3 to 0.8
- out_gain: float32 [128], replicated, may hold values from 0.1 to 1.9
Outputs:
- query_grad: float32 [4096, 1024], P('sp', 'tp')
- key_grad: float32 [4096, 1024], P('sp', 'tp')
- value_grad: float32 [4096, 1024], P('sp', 'tp')
- weight_grad: float32 [2048, 1024], P('sp', 'tp')
Inputs may be any that keep to these rules, and one draw needn't show every extreme that they name: `log_sums`: each entry is the logarithm of the sum of exp(scores_c[t, s]) over s <= t for its row t, head h and map c.
All inputs are finite; a program needn't handle non-finite values.
Results may differ from a plain program's by a relative error of at most 0.008.
Values may be sent and summed in bfloat16 or wider, within the bound.
A program may use at most 64 MiB of HBM per device.

v0:
```python
import jax
import jax.numpy as jnp
from jax import lax
from jax.sharding import PartitionSpec as P

norm_floor = 0.25
block_rows = 512


def head_cotangent(out_pair, cotangent, lambdas, out_gain):
    tok_rows = out_pair.shape[0]
    head_count = lambdas.shape[0]
    out_maps = out_pair.astype(jnp.float32).reshape(tok_rows, head_count, 2, -1)
    lam_cols = lambdas[None, :, None]
    merged = out_maps[:, :, 0] - lam_cols * out_maps[:, :, 1]
    inv_norm = lax.rsqrt(jnp.mean(merged * merged, axis=-1, keepdims=True) + norm_floor)
    scaled = cotangent.astype(jnp.float32).reshape(merged.shape) * out_gain
    inner_dot = jnp.mean(scaled * merged, axis=-1, keepdims=True)
    out_grad = (inv_norm * scaled - merged * (inv_norm * inv_norm * inv_norm) * inner_dot).astype(
        jnp.bfloat16
    )
    grad_wide = out_grad.astype(jnp.float32)
    first_map = jnp.sum(grad_wide * out_maps[:, :, 0], axis=-1)
    second_map = -lambdas[None, :] * jnp.sum(grad_wide * out_maps[:, :, 1], axis=-1)
    return (out_grad, jnp.stack([first_map, second_map], axis=-1))


def block_terms(
    query_block,
    key_block,
    value_block,
    grad_block,
    log_block,
    term_block,
    lambdas,
    query_pos,
    key_pos,
):
    factor = query_block.shape[-1] ** (-0.5)
    scores = (
        jnp.einsum("qhcd,khcd->hcqk", query_block, key_block, preferred_element_type=jnp.float32)
        * factor
    )
    visible = key_pos[None, :] <= query_pos[:, None]
    shifted = scores - jnp.transpose(log_block, (1, 2, 0))[..., None]
    softmax_maps = jnp.where(visible, jnp.exp(shifted), 0.0)
    value_dot = jnp.einsum(
        "qhe,khe->hqk", grad_block, value_block, preferred_element_type=jnp.float32
    )
    lam_cols = lambdas[:, None, None]
    weights = (softmax_maps[:, 0] - lam_cols * softmax_maps[:, 1]).astype(jnp.bfloat16)
    term_cols = jnp.transpose(term_block, (1, 2, 0))
    first_map = softmax_maps[:, 0] * (value_dot - term_cols[:, 0, :, None])
    second_map = softmax_maps[:, 1] * (-lam_cols * value_dot - term_cols[:, 1, :, None])
    dscore = (jnp.stack([first_map, second_map], axis=1) * factor).astype(jnp.bfloat16)
    return (weights, dscore)


def block_span():
    return block_rows


def per_device(
    queries, key_vectors, latents, w_value, log_sums, out_pair, cotangent, lambdas, out_gain
):
    tok_rows = queries.shape[0]
    head_count = lambdas.shape[0]
    offset = lax.axis_index("sp") * tok_rows
    own_pos = offset + jnp.arange(tok_rows, dtype=jnp.int32)
    last_pos = offset + tok_rows - 1
    gathered = lax.all_gather(latents, "tp", axis=1, tiled=True)
    values = jnp.dot(gathered, w_value, preferred_element_type=jnp.float32).astype(jnp.bfloat16)
    out_grad, row_terms = head_cotangent(out_pair, cotangent, lambdas, out_gain)
    query_heads = queries.reshape(tok_rows, head_count, 2, -1)
    key_heads = key_vectors.reshape(tok_rows, head_count, 2, -1)
    value_heads = values.reshape(tok_rows, head_count, -1)
    log_heads = log_sums.reshape(tok_rows, head_count, 2)
    grad_flat = out_grad.reshape(tok_rows, -1)
    term_flat = row_terms.reshape(tok_rows, -1)
    zero_keys = jnp.zeros(key_heads.shape, jnp.float32)
    zero_values = jnp.zeros(value_heads.shape, jnp.float32)
    shards = (
        lax.all_gather(key_vectors, "sp", axis=0, tiled=True),
        lax.all_gather(values, "sp", axis=0, tiled=True),
    )
    key_piece = shards[0]
    value_piece = shards[1]
    piece_rows = key_piece.shape[0]
    block_len = block_span()

    def query_add_block(block_idx, partial_value):
        begin_row = block_idx * block_len
        key_block = lax.dynamic_slice_in_dim(key_piece, begin_row, block_len, 0).reshape(
            block_len, head_count, 2, -1
        )
        value_block = lax.dynamic_slice_in_dim(value_piece, begin_row, block_len, 0).reshape(
            block_len, head_count, -1
        )
        key_pos = begin_row + jnp.arange(block_len, dtype=jnp.int32)

        def query_compute(sums):
            weights, dscore = block_terms(
                query_heads,
                key_block,
                value_block,
                out_grad,
                log_heads,
                row_terms,
                lambdas,
                own_pos,
                key_pos,
            )
            return sums + jnp.einsum(
                "hcqk,khcd->qhcd", dscore, key_block, preferred_element_type=jnp.float32
            )

        return lax.cond(begin_row <= last_pos, query_compute, lambda sums: sums, partial_value)

    query_grad = lax.fori_loop(0, piece_rows // block_len, query_add_block, zero_keys)
    shards = (
        lax.all_gather(queries.astype(jnp.float32), "sp", axis=0, tiled=True).astype(jnp.bfloat16),
        lax.all_gather(grad_flat.astype(jnp.float32), "sp", axis=0, tiled=True).astype(
            jnp.bfloat16
        ),
        lax.all_gather(log_sums, "sp", axis=0, tiled=True),
        lax.all_gather(term_flat, "sp", axis=0, tiled=True),
    )
    query_piece = shards[0]
    grad_piece = shards[1]
    log_piece = shards[2]
    term_piece = shards[3]
    piece_rows = query_piece.shape[0]
    key_block_len = block_span()

    def key_add_block(block_idx, partial_value):
        begin_row = block_idx * key_block_len
        query_block = lax.dynamic_slice_in_dim(query_piece, begin_row, key_block_len, 0).reshape(
            key_block_len, head_count, 2, -1
        )
        grad_block = lax.dynamic_slice_in_dim(grad_piece, begin_row, key_block_len, 0).reshape(
            key_block_len, head_count, -1
        )
        log_block = lax.dynamic_slice_in_dim(log_piece, begin_row, key_block_len, 0).reshape(
            key_block_len, head_count, 2
        )
        term_block = lax.dynamic_slice_in_dim(term_piece, begin_row, key_block_len, 0).reshape(
            key_block_len, head_count, 2
        )
        query_pos = begin_row + jnp.arange(key_block_len, dtype=jnp.int32)

        def key_compute(sums):
            weights, dscore = block_terms(
                query_block,
                key_heads,
                value_heads,
                grad_block,
                log_block,
                term_block,
                lambdas,
                query_pos,
                own_pos,
            )
            key_sum = sums[0] + jnp.einsum(
                "hcqk,qhcd->khcd", dscore, query_block, preferred_element_type=jnp.float32
            )
            value_sum = sums[1] + jnp.einsum(
                "hqk,qhe->khe", weights, grad_block, preferred_element_type=jnp.float32
            )
            return (key_sum, value_sum)

        return lax.cond(
            begin_row + key_block_len - 1 >= offset, key_compute, lambda sums: sums, partial_value
        )

    key_grad, value_grad = lax.fori_loop(
        0, piece_rows // key_block_len, key_add_block, (zero_keys, zero_values)
    )
    value_flat = value_grad.reshape(tok_rows, -1)
    value_narrow = value_flat.astype(jnp.bfloat16)
    weight_grad = lax.psum_scatter(
        lax.dot_general(
            gathered, value_narrow, (((0,), (0,)), ((), ())), preferred_element_type=jnp.float32
        ),
        "sp",
        scatter_dimension=0,
        tiled=True,
    )
    return (
        query_grad.reshape(tok_rows, -1),
        key_grad.reshape(tok_rows, -1),
        value_flat,
        weight_grad,
    )


def solution(mesh):
    return jax.shard_map(
        per_device,
        mesh=mesh,
        in_specs=(
            P("sp", "tp"),
            P("sp", "tp"),
            P("sp", "tp"),
            P(None, "tp"),
            P("sp", "tp"),
            P("sp", "tp"),
            P("sp", "tp"),
            P("tp"),
            P(),
        ),
        out_specs=(P("sp", "tp"), P("sp", "tp"), P("sp", "tp"), P("sp", "tp")),
        check_vma=False,
    )
```

profile of v0, /device:TPU:0, one launch (start us, length us, event | category | flops | bytes accessed | tf_op | source)
XLA Modules:
  0.0 320.5 jit_solution(6820730226512585887)
XLA Ops:
  14.8 20.2 %all-gather.8.cloned.1.call-done = bf16[512,2048]{1,0:T(8,128)(2,1)} async-done(((bf16[512,512]{1,0:T(8,128)(2,1)}), bf16[512,2048]{1,0:T(8,128)(2,1)}) %all-gather.8.cloned.1.call-update) | async-done | bytes 2097168 | tf_op jit(solution)/shard_map/all_gather | solution.py:71
  38.7 31.0 %all_gather.25 = f32[4096,4]{0,1:T(4,128)S(1)} all-gather(f32[512,4]{0,1:T(4,128)S(1)} %copy-done.6), channel_id=1, replica_groups=mesh['sp'=8,'tp'=4] {'sp'}, dimensions={0}, use_global_device_ids=true | all-gather | bytes 73728 | tf_op jit(solution)/shard_map/all_gather | solution.py:125
  69.7 31.9 %all_gather.27 = f32[4096,4]{0,1:T(4,128)} all-gather(f32[512,4]{0,1:T(4,128)S(1)} %reshape.188), channel_id=1, replica_groups=mesh['sp'=8,'tp'=4] {'sp'}, dimensions={0}, use_global_device_ids=true | all-gather | bytes 73728 | tf_op jit(solution)/shard_map/all_gather | solution.py:126
  102.8 37.0 %all-gather.14.cloned.1.call-done = bf16[4096,256]{0,1:T(8,128)(2,1)} async-done(((bf16[512,256]{0,1:T(8,128)(2,1)}), bf16[4096,256]{0,1:T(8,128)(2,1)}) %all-gather.14.cloned.1.call-update) | async-done | bytes 2097168 | tf_op jit(solution)/shard_map/all_gather | solution.py:122
  139.9 90.7 %while.39 = (s32[]{:T(128)}, f32[512,2,2,64]{0,3,2,1:T(8,128)S(1)}, f32[512,2,128]{2,0,1:T(8,128)S(1)}, s32[]{:T(128)}, bf16[4096,256]{0,1:T(8,128)(2,1)}, /*ind...) while((s32[]{:T(128)}, f32[512,2,2,64]{0,3,2,1:T(8,128)S(1)}, ...), condition=%wide.region_11.12_spmd.clone.clone, body=%wide.region_8.11_spmd.clone.clone.sunk | while | flops 547881984 | bytes 43121072 | solution.py:175
  140.0 11.3 %conditional.8 = ((f32[512,2,2,64]{0,3,2,1:T(8,128)S(1)}, f32[512,2,128]{2,0,1:T(8,128)S(1)})) conditional(s32[]{:T(128)} %convert_element_type.110, (f32[512,2,2,64]{0,3,2,1:T(8,128)S(1)}, f32[512,2,128]{2,0,1:T(8,128)S(1)}) %tuple.152, (s32[]{:T(128)}, s32[]{:T(128)}, s32[512]{0:T(512)S(1)}, bf16[4096,256]{0,1:T(8,128)(2,1)}, ...), branch_computations={%region_9.9_spmd, %region_10.10_spmd} | conditional | flops 547881984 | bytes 43118728 | solution.py:171
  142.0 3.2 exponential_select_fusion
  151.3 11.3 %conditional.8 = ((f32[512,2,2,64]{0,3,2,1:T(8,128)S(1)}, f32[512,2,128]{2,0,1:T(8,128)S(1)})) conditional(s32[]{:T(128)} %convert_element_type.110, (f32[512,2,2,64]{0,3,2,1:T(8,128)S(1)}, f32[512,2,128]{2,0,1:T(8,128)S(1)}) %tuple.152, (s32[]{:T(128)}, s32[]{:T(128)}, s32[512]{0:T(512)S(1)}, bf16[4096,256]{0,1:T(8,128)(2,1)}, ...), branch_computations={%region_9.9_spmd, %region_10.10_spmd} | conditional | flops 547881984 | bytes 43118728 | solution.py:171
  162.6 11.4 %conditional.8 = ((f32[512,2,2,64]{0,3,2,1:T(8,128)S(1)}, f32[512,2,128]{2,0,1:T(8,128)S(1)})) conditional(s32[]{:T(128)} %convert_element_type.110, (f32[512,2,2,64]{0,3,2,1:T(8,128)S(1)}, f32[512,2,128]{2,0,1:T(8,128)S(1)}) %tuple.152, (s32[]{:T(128)}, s32[]{:T(128)}, s32[512]{0:T(512)S(1)}, bf16[4096,256]{0,1:T(8,128)(2,1)}, ...), branch_computations={%region_9.9_spmd, %region_10.10_spmd} | conditional | flops 547881984 | bytes 43118728 | solution.py:171
  164.7 3.2 exponential_select_fusion
  174.1 11.3 %conditional.8 = ((f32[512,2,2,64]{0,3,2,1:T(8,128)S(1)}, f32[512,2,128]{2,0,1:T(8,128)S(1)})) conditional(s32[]{:T(128)} %convert_element_type.110, (f32[512,2,2,64]{0,3,2,1:T(8,128)S(1)}, f32[512,2,128]{2,0,1:T(8,128)S(1)}) %tuple.152, (s32[]{:T(128)}, s32[]{:T(128)}, s32[512]{0:T(512)S(1)}, bf16[4096,256]{0,1:T(8,128)(2,1)}, ...), branch_computations={%region_9.9_spmd, %region_10.10_spmd} | conditional | flops 547881984 | bytes 43118728 | solution.py:171
  176.1 3.2 exponential_select_fusion
  185.4 11.2 %conditional.8 = ((f32[512,2,2,64]{0,3,2,1:T(8,128)S(1)}, f32[512,2,128]{2,0,1:T(8,128)S(1)})) conditional(s32[]{:T(128)} %convert_element_type.110, (f32[512,2,2,64]{0,3,2,1:T(8,128)S(1)}, f32[512,2,128]{2,0,1:T(8,128)S(1)}) %tuple.152, (s32[]{:T(128)}, s32[]{:T(128)}, s32[512]{0:T(512)S(1)}, bf16[4096,256]{0,1:T(8,128)(2,1)}, ...), branch_computations={%region_9.9_spmd, %region_10.10_spmd} | conditional | flops 547881984 | bytes 43118728 | solution.py:171
  187.4 3.2 exponential_select_fusion
  196.7 11.3 %conditional.8 = ((f32[512,2,2,64]{0,3,2,1:T(8,128)S(1)}, f32[512,2,128]{2,0,1:T(8,128)S(1)})) conditional(s32[]{:T(128)} %convert_element_type.110, (f32[512,2,2,64]{0,3,2,1:T(8,128)S(1)}, f32[512,2,128]{2,0,1:T(8,128)S(1)}) %tuple.152, (s32[]{:T(128)}, s32[]{:T(128)}, s32[512]{0:T(512)S(1)}, bf16[4096,256]{0,1:T(8,128)(2,1)}, ...), branch_computations={%region_9.9_spmd, %region_10.10_spmd} | conditional | flops 547881984 | bytes 43118728 | solution.py:171
  208.0 11.2 %conditional.8 = ((f32[512,2,2,64]{0,3,2,1:T(8,128)S(1)}, f32[512,2,128]{2,0,1:T(8,128)S(1)})) conditional(s32[]{:T(128)} %convert_element_type.110, (f32[512,2,2,64]{0,3,2,1:T(8,128)S(1)}, f32[512,2,128]{2,0,1:T(8,128)S(1)}) %tuple.152, (s32[]{:T(128)}, s32[]{:T(128)}, s32[512]{0:T(512)S(1)}, bf16[4096,256]{0,1:T(8,128)(2,1)}, ...), branch_computations={%region_9.9_spmd, %region_10.10_spmd} | conditional | flops 547881984 | bytes 43118728 | solution.py:171
  210.1 3.2 exponential_select_fusion
  219.3 11.3 %conditional.8 = ((f32[512,2,2,64]{0,3,2,1:T(8,128)S(1)}, f32[512,2,128]{2,0,1:T(8,128)S(1)})) conditional(s32[]{:T(128)} %convert_element_type.110, (f32[512,2,2,64]{0,3,2,1:T(8,128)S(1)}, f32[512,2,128]{2,0,1:T(8,128)S(1)}) %tuple.152, (s32[]{:T(128)}, s32[]{:T(128)}, s32[512]{0:T(512)S(1)}, bf16[4096,256]{0,1:T(8,128)(2,1)}, ...), branch_computations={%region_9.9_spmd, %region_10.10_spmd} | conditional | flops 547881984 | bytes 43118728 | solution.py:171
  221.4 3.2 exponential_select_fusion
  230.7 3.9 %convolution_bitcast_fusion.1 = f32[2048,256]{0,1:T(8,128)} fusion(bf16[512,2048]{1,0:T(8,128)(2,1)} %all-gather.8.cloned.1.call-done, f32[512,256]{1,0:T(8,128)S(1)} %copy_bitcast_fusion.2), kind=kOutput, calls=%fused_computation.46 | convolution fusion | flops 537001984 | bytes 4718592 | tf_op jit(solution)/shard_map/dot_general | solution.py:181
  235.8 5.5 %all-gather.10.cloned.1.call-done = bf16[4096,256]{0,1:T(8,128)(2,1)} async-done(((bf16[512,256]{0,1:T(8,128)(2,1)}), bf16[4096,256]{0,1:T(8,128)(2,1)}) %all-gather.10.cloned.1.call-update) | async-done | bytes 2097168 | tf_op jit(solution)/shard_map/all_gather | solution.py:84
  241.4 4.3 %while.38 = (s32[]{:T(128)}, f32[512,2,2,64]{0,3,2,1:T(8,128)S(1)}, s32[]{:T(128)}, bf16[4096,256]{0,1:T(8,128)(2,1)}, bf16[512,2,2,64]{0,3,2,1:T(8,128)(2,1)S(1...) while((s32[]{:T(128)}, f32[512,2,2,64]{0,3,2,1:T(8,128)S(1)}, ...), condition=%wide.region_7.8_spmd.clone, body=%wide.region_4.7_spmd.clone.sunk | while | flops 411960320 | bytes 20756812 | solution.py:119
  241.4 3.9 %conditional.7 = (f32[512,2,2,64]{0,3,2,1:T(8,128)S(1)}) conditional(s32[]{:T(128)} %convert_element_type.109, f32[512,2,2,64]{0,3,2,1:T(8,128)S(1)} %get-tuple-element.1245, (s32[]{:T(128)}, s32[512]{0:T(512)S(1)}, s32[]{:T(128)}, bf16[4096,256]{0,1:T(8,128)(2,1)}, bf16[512,2,2,64]{0,3,2,1:T(8,128)(2,1)S(1)}, /*index=5*/f32[512,2,2]{0,2,1:T(2,128)S(1)}, ...), branch_computations={%region_5.0_spmd, %region_6.6_spmd} | conditional | flops 411960320 | bytes 20754510 | solution.py:117
  246.7 65.2 %reduce-scatter.2.cloned.1.call-done = f32[256,256]{0,1:T(8,128)} async-done(((f32[2048,256]{0,1:T(8,128)}), f32[256,256]{0,1:T(8,128)}) %reduce-scatter.2.cloned.1.call-update) | async-done | bytes 262160 | tf_op jit(solution)/shard_map/reduce_scatter | solution.py:180
  (210 shorter events, 91.0 us)
Async XLA Ops:
  7.2 27.7 %copy-start = (bf16[2048,256]{1,0:T(8,128)(2,1)S(1)}, bf16[2048,256]{1,0:T(8,128)(2,1)}, u32[]{:S(2)}) copy-start(bf16[2048,256]{1,0:T(8,128)(2,1)} %param.20) | copy-start | bytes 3145732
  7.2 3.9 %copy-start.5 = (bf16[512,256]{1,0:T(8,128)(2,1)S(1)}, bf16[512,256]{1,0:T(8,128)(2,1)}, u32[]{:S(2)}) copy-start(bf16[512,256]{1,0:T(8,128)(2,1)} %param.23) | copy-start | bytes 786436
  7.2 4.1 %copy-start.8 = (f32[128]{0:T(128)S(1)}, f32[128]{0:T(128)}, u32[]{:S(2)}) copy-start(f32[128]{0:T(128)} %param.25) | copy-start | bytes 1540
  7.2 4.1 %copy-start.7 = (f32[2]{0:T(128)S(1)}, f32[2]{0:T(128)}, u32[]{:S(2)}) copy-start(f32[2]{0:T(128)} %param.24) | copy-start | bytes 28
  7.2 27.7 %all-gather.8.cloned.1.call-start = ((), (), s32[]{:S(2)}) async-start(), calls=%async_computation.2 | async-start | bytes 2621440 | tf_op jit(solution)/shard_map/all_gather | solution.py:71
  7.9 94.8 %all-gather.12.cloned.1.call-start = ((), (), s32[]{:S(2)}) async-start(), calls=%async_computation.4 | async-start | bytes 2359296 | tf_op jit(solution)/shard_map/all_gather | solution.py:121
  9.8 130.0 %all-gather.14.cloned.1.call-start = ((), (), s32[]{:S(2)}) async-start(), calls=%async_computation.5 | async-start | bytes 2359296 | tf_op jit(solution)/shard_map/all_gather | solution.py:122
  12.8 222.9 %all-gather.6.cloned.1.call-start = ((), (), s32[]{:S(2)}) async-start(), calls=%async_computation.1 | async-start | bytes 2359296 | tf_op jit(solution)/shard_map/all_gather | solution.py:83
  14.7 226.6 %all-gather.10.cloned.1.call-start = ((), (), s32[]{:S(2)}) async-start(), calls=%async_computation.3 | async-start | bytes 2359296 | tf_op jit(solution)/shard_map/all_gather | solution.py:84
  38.0 0.7 copy-start.6
  38.0 101.9 %copy-start.4 = (bf16[512,256]{0,1:T(8,128)(2,1)S(1)}, bf16[512,256]{0,1:T(8,128)(2,1)}, u32[]{:S(2)}) copy-start(bf16[512,256]{0,1:T(8,128)(2,1)} %copy.47) | copy-start | bytes 786436
  38.0 273.8 %reduce-scatter.2.cloned.1.call-start = ((), (), s32[]{:S(2)}) async-start(), calls=%async_computation.6 | async-start | bytes 2359296 | tf_op jit(solution)/shard_map/reduce_scatter | solution.py:180
  148.2 2.3 copy-start.1
  159.6 2.2 copy-start.1
  171.0 2.2 copy-start.1
  182.3 2.2 copy-start.1
  193.6 2.2 copy-start.1
  204.9 2.2 copy-start.1
  216.2 2.2 copy-start.1
  227.6 2.2 copy-start.1
  230.7 3.9 %copy-start.2 = (f32[512,256]{1,0:T(8,128)}, f32[512,256]{1,0:T(8,128)S(1)}, u32[]{:S(2)}) copy-start(f32[512,256]{1,0:T(8,128)S(1)} %copy_bitcast_fusion.2) | copy-start | bytes 1572868
  234.6 6.8 %copy-start.3 = (bf16[512,256]{0,1:T(8,128)(2,1)S(1)}, bf16[512,256]{0,1:T(8,128)(2,1)}, u32[]{:S(2)}) copy-start(bf16[512,256]{0,1:T(8,128)(2,1)} %copy.48) | copy-start | bytes 786436
Sparse Core Ops, SparseCore 0:
  9.6 25.2 all-gather.7
  37.5 50.9 all-gather.11
  91.1 48.6 all-gather.13
  142.3 48.5 all-gather.5
  192.7 48.5 all-gather.9
  244.7 67.0 reduce-scatter.1
where the time goes:
time: 322 us; the launch traced here: 320 us
  waiting for transfers between devices  129 us (40%)
  matrix products  69.3 us (22%)
  blocking collectives  62.9 us (20%)
  local copies, waits for them, and re-layouts  39.8 us (12%)
  between operations  14.3 us (4%)
  other arithmetic  3.63 us (1%)
    reduce_scatter x1, waiting for transfers between devices, per_device(): lax.psum_scatter(lax.dot_general(gathered, value_narrow, (((0,), (0,)), (...  65.2 us
    all_gather x1, waiting for transfers between devices, per_device(): lax.all_gather(grad_flat.astype(jnp.float32), 'sp', axis=0, tiled=True)  37 us
    all_gather x1, blocking collectives, per_device(): lax.all_gather(term_flat, 'sp', axis=0, tiled=True)  31.9 us
    all_gather x1, blocking collectives, per_device(): lax.all_gather(log_sums, 'sp', axis=0, tiled=True)  31 us
    dot_general x9, matrix products, block_terms(): jnp.einsum('qhcd,khcd->hcqk', query_block, key_block, preferred_element_t...  26.6 us
    dot_general x9, matrix products, block_terms(): jnp.einsum('qhe,khe->hqk', grad_block, value_block, preferred_element_typ...  24.4 us
    all_gather x1, waiting for transfers between devices, per_device(): gathered = lax.all_gather(latents, 'tp', axis=1, tiled=True)  20.2 us
    cond x32, local copies, waits for them, and re-layouts  13.3 us
  transfers between devices with their start and end apart: 6, of which 4 were waited for; matrix products, arithmetic and copies ran while one was open for 30% of the time, Pallas kernels for 0%

commit v1 on v0

--- a/solution.py
+++ b/solution.py
@@ -68,7 +68,13 @@
     offset = lax.axis_index("sp") * tok_rows
     own_pos = offset + jnp.arange(tok_rows, dtype=jnp.int32)
     last_pos = offset + tok_rows - 1
-    gathered = lax.all_gather(latents, "tp", axis=1, tiled=True)
+    size = lax.axis_size("tp")
+    held, blocks = (latents, [latents])
+    for _ in range(size - 1):
+        held = lax.ppermute(held, "tp", [(i, (i + 1) % size) for i in range(size)])
+        blocks.insert(0, held)
+    line = jnp.concatenate(blocks, axis=1)
+    gathered = jnp.roll(line, (lax.axis_index("tp") + 1) * latents.shape[1], axis=1)
     values = jnp.dot(gathered, w_value, preferred_element_type=jnp.float32).astype(jnp.bfloat16)
     out_grad, row_terms = head_cotangent(out_pair, cotangent, lambdas, out_gain)
     query_heads = queries.reshape(tok_rows, head_count, 2, -1)

time: 322 us -> 295 us (0.916)
  waiting for transfers between devices: 129 us -> 100 us
    all_gather x1, waiting for transfers between devices: 37 us -> 0.02 us  [per_device(): lax.all_gather(grad_flat.astype(jnp.float32), 'sp', axis=0, tiled=True)]
    ppermute x0 -> x3, waiting for transfers between devices: none -> 26.4 us  [per_device(): held = lax.ppermute(held, 'tp', [(i, (i + 1) % size) for i in range(size)])]
    all_gather x1 -> x0, waiting for transfers between devices: 20.2 us -> none  [per_device(): gathered = lax.all_gather(latents, 'tp', axis=1, tiled=True)]
    unnamed x25 -> x43, local copies, waits for them, and re-layouts: 10.3 us -> 16.7 us
    dynamic_slice x8, local copies, waits for them, and re-layouts: 5.66 us -> 0.09 us  [key_add_block(): lax.dynamic_slice_in_dim(term_piece, begin_row, key_block_len, 0)]
    cond x32 -> x48, local copies, waits for them, and re-layouts: 13.3 us -> 13.3 us
  transfers between devices with their start and end apart: 6 -> 8, of which waited for: 4 -> 5; matrix products, arithmetic and copies ran while one was open for 30% -> 32% of each run, Pallas kernels for 0% -> 0%
where the time goes in v1:
time: 295 us; the launch traced here: 294 us
  waiting for transfers between devices  100 us (34%)
  matrix products  68.4 us (23%)
  blocking collectives  63.8 us (22%)
  local copies, waits for them, and re-layouts  40.6 us (14%)
  between operations  14.1 us (5%)
  other arithmetic  4.34 us (1%)
    reduce_scatter x1, waiting for transfers between devices, per_device(): lax.psum_scatter(lax.dot_general(gathered, value_narrow, (((0,), (0,)), (...  65.1 us
    all_gather x1, blocking collectives, per_device(): lax.all_gather(log_sums, 'sp', axis=0, tiled=True)  32.5 us
    all_gather x1, blocking collectives, per_device(): lax.all_gather(term_flat, 'sp', axis=0, tiled=True)  31.3 us
    dot_general x9, matrix products, block_terms(): jnp.einsum('qhcd,khcd->hcqk', query_block, key_block, preferred_element_t...  27.2 us
    ppermute x3, waiting for transfers between devices, per_device(): held = lax.ppermute(held, 'tp', [(i, (i + 1) % size) for i in range(size)])  26.4 us
    dot_general x9, matrix products, block_terms(): jnp.einsum('qhe,khe->hqk', grad_block, value_block, preferred_element_typ...  24.4 us
    unnamed x43, local copies, waits for them, and re-layouts  16.7 us
    cond x48, local copies, waits for them, and re-layouts  13.3 us
  transfers between devices with their start and end apart: 8, of which 5 were waited for; matrix products, arithmetic and copies ran while one was open for 32% of the time, Pallas kernels for 0%

profile of v1, /device:TPU:0, one launch (start us, length us, event | category | flops | bytes accessed | tf_op | source)
XLA Modules:
  0.0 293.8 jit_solution(17803534033266157389)
XLA Ops:
  15.6 8.8 %collective-permute-done = bf16[512,512]{1,0:T(8,128)(2,1)S(1)} collective-permute-done((bf16[512,512]{1,0:T(8,128)(2,1)S(1)}, bf16[512,512]{1,0:T(8,128)(2,1)S(1)}, u32[]{:S(2)}, u32[]{:S(2)}) %collective-permute-start) | collective-permute-done | bytes 524320 | tf_op jit(solution)/shard_map/ppermute | solution.py:74
  25.2 8.7 %collective-permute-done.1 = bf16[512,512]{1,0:T(8,128)(2,1)} collective-permute-done((bf16[512,512]{1,0:T(8,128)(2,1)S(1)}, bf16[512,512]{1,0:T(8,128)(2,1)}, u32[]{:S(2)}, u32[]{:S(2)}) %collective-permute-start.1) | collective-permute-done | bytes 524320 | tf_op jit(solution)/shard_map/ppermute | solution.py:74
  33.9 8.9 %collective-permute-done.2 = bf16[512,512]{1,0:T(8,128)(2,1)} collective-permute-done((bf16[512,512]{1,0:T(8,128)(2,1)}, bf16[512,512]{1,0:T(8,128)(2,1)}, u32[]{:S(2)}, u32[]{:S(2)}) %collective-permute-start.2) | collective-permute-done | bytes 524320 | tf_op jit(solution)/shard_map/ppermute | solution.py:74
  52.2 32.5 %all_gather.21 = f32[4096,4]{0,1:T(4,128)S(1)} all-gather(f32[512,4]{0,1:T(4,128)S(1)} %copy-done.11), channel_id=1, replica_groups=mesh['sp'=8,'tp'=4] {'sp'}, dimensions={0}, use_global_device_ids=true | all-gather | bytes 73728 | tf_op jit(solution)/shard_map/all_gather | solution.py:131
  84.7 31.3 %all_gather.23 = f32[4096,4]{0,1:T(4,128)S(1)} all-gather(f32[512,4]{0,1:T(4,128)S(1)} %reshape.188), channel_id=1, replica_groups=mesh['sp'=8,'tp'=4] {'sp'}, dimensions={0}, use_global_device_ids=true | all-gather | bytes 73728 | tf_op jit(solution)/shard_map/all_gather | solution.py:132
  116.4 85.9 %while.39 = (s32[]{:T(128)}, f32[512,2,2,64]{0,3,2,1:T(8,128)S(1)}, f32[512,2,128]{2,0,1:T(8,128)S(1)}, s32[]{:T(128)}, bf16[4096,256]{0,1:T(8,128)(2,1)}, /*ind...) while((s32[]{:T(128)}, f32[512,2,2,64]{0,3,2,1:T(8,128)S(1)}, ...), condition=%wide.region_11.12_spmd.clone.clone, body=%wide.region_8.11_spmd.clone.clone.sunk | while | flops 547881984 | bytes 43121128 | solution.py:181
  116.4 10.8 %conditional.8 = ((f32[512,2,2,64]{0,3,2,1:T(8,128)S(1)}, f32[512,2,128]{2,0,1:T(8,128)S(1)})) conditional(s32[]{:T(128)} %convert_element_type.110, (f32[512,2,2,64]{0,3,2,1:T(8,128)S(1)}, f32[512,2,128]{2,0,1:T(8,128)S(1)}) %tuple.151, (s32[]{:T(128)}, s32[]{:T(128)}, s32[512]{0:T(512)S(1)}, bf16[4096,256]{0,1:T(8,128)(2,1)}, ...), branch_computations={%region_9.9_spmd, %region_10.10_spmd} | conditional | flops 547881984 | bytes 43118784 | solution.py:177
  127.2 10.7 %conditional.8 = ((f32[512,2,2,64]{0,3,2,1:T(8,128)S(1)}, f32[512,2,128]{2,0,1:T(8,128)S(1)})) conditional(s32[]{:T(128)} %convert_element_type.110, (f32[512,2,2,64]{0,3,2,1:T(8,128)S(1)}, f32[512,2,128]{2,0,1:T(8,128)S(1)}) %tuple.151, (s32[]{:T(128)}, s32[]{:T(128)}, s32[512]{0:T(512)S(1)}, bf16[4096,256]{0,1:T(8,128)(2,1)}, ...), branch_computations={%region_9.9_spmd, %region_10.10_spmd} | conditional | flops 547881984 | bytes 43118784 | solution.py:177
  137.9 10.8 %conditional.8 = ((f32[512,2,2,64]{0,3,2,1:T(8,128)S(1)}, f32[512,2,128]{2,0,1:T(8,128)S(1)})) conditional(s32[]{:T(128)} %convert_element_type.110, (f32[512,2,2,64]{0,3,2,1:T(8,128)S(1)}, f32[512,2,128]{2,0,1:T(8,128)S(1)}) %tuple.151, (s32[]{:T(128)}, s32[]{:T(128)}, s32[512]{0:T(512)S(1)}, bf16[4096,256]{0,1:T(8,128)(2,1)}, ...), branch_computations={%region_9.9_spmd, %region_10.10_spmd} | conditional | flops 547881984 | bytes 43118784 | solution.py:177
  139.3 3.2 %exponential_select_fusion = f32[2,2,512,512]{3,2,1,0:T(8,128)} fusion(bf16[512,2,2,64]{0,3,2,1:T(8,128)(2,1)S(1)} %bitcast.167, bf16[512,2,2,64]{0,3,2,1:T(8,128)(2,1)S(1)} %get-tuple-element.842, f32[2,2,512]{2,1,0:T(2,128)S(1)} %bitcast.180, pred[512,512]{1,0:T(8,128)(4,1)S(1)} %broadcast_compare_fusion.1), kind=kOutput, calls=%fused_computation.24 | convolution fusion | flops 137363456 | bytes 4988928 | tf_op jit(solution)/shard_map/while/body/eval_jaxpr/cond/branch_1_fun/qhcd,khcd->hcqk/dot_general | solution.py:41
  148.8 10.7 %conditional.8 = ((f32[512,2,2,64]{0,3,2,1:T(8,128)S(1)}, f32[512,2,128]{2,0,1:T(8,128)S(1)})) conditional(s32[]{:T(128)} %convert_element_type.110, (f32[512,2,2,64]{0,3,2,1:T(8,128)S(1)}, f32[512,2,128]{2,0,1:T(8,128)S(1)}) %tuple.151, (s32[]{:T(128)}, s32[]{:T(128)}, s32[512]{0:T(512)S(1)}, bf16[4096,256]{0,1:T(8,128)(2,1)}, ...), branch_computations={%region_9.9_spmd, %region_10.10_spmd} | conditional | flops 547881984 | bytes 43118784 | solution.py:177
  150.2 3.2 %exponential_select_fusion = f32[2,2,512,512]{3,2,1,0:T(8,128)} fusion(bf16[512,2,2,64]{0,3,2,1:T(8,128)(2,1)S(1)} %bitcast.167, bf16[512,2,2,64]{0,3,2,1:T(8,128)(2,1)S(1)} %get-tuple-element.842, f32[2,2,512]{2,1,0:T(2,128)S(1)} %bitcast.180, pred[512,512]{1,0:T(8,128)(4,1)S(1)} %broadcast_compare_fusion.1), kind=kOutput, calls=%fused_computation.24 | convolution fusion | flops 137363456 | bytes 4988928 | tf_op jit(solution)/shard_map/while/body/eval_jaxpr/cond/branch_1_fun/qhcd,khcd->hcqk/dot_general | solution.py:41
  159.5 10.7 %conditional.8 = ((f32[512,2,2,64]{0,3,2,1:T(8,128)S(1)}, f32[512,2,128]{2,0,1:T(8,128)S(1)})) conditional(s32[]{:T(128)} %convert_element_type.110, (f32[512,2,2,64]{0,3,2,1:T(8,128)S(1)}, f32[512,2,128]{2,0,1:T(8,128)S(1)}) %tuple.151, (s32[]{:T(128)}, s32[]{:T(128)}, s32[512]{0:T(512)S(1)}, bf16[4096,256]{0,1:T(8,128)(2,1)}, ...), branch_computations={%region_9.9_spmd, %region_10.10_spmd} | conditional | flops 547881984 | bytes 43118784 | solution.py:177
  160.9 3.2 %exponential_select_fusion = f32[2,2,512,512]{3,2,1,0:T(8,128)} fusion(bf16[512,2,2,64]{0,3,2,1:T(8,128)(2,1)S(1)} %bitcast.167, bf16[512,2,2,64]{0,3,2,1:T(8,128)(2,1)S(1)} %get-tuple-element.842, f32[2,2,512]{2,1,0:T(2,128)S(1)} %bitcast.180, pred[512,512]{1,0:T(8,128)(4,1)S(1)} %broadcast_compare_fusion.1), kind=kOutput, calls=%fused_computation.24 | convolution fusion | flops 137363456 | bytes 4988928 | tf_op jit(solution)/shard_map/while/body/eval_jaxpr/cond/branch_1_fun/qhcd,khcd->hcqk/dot_general | solution.py:41
  170.2 10.7 %conditional.8 = ((f32[512,2,2,64]{0,3,2,1:T(8,128)S(1)}, f32[512,2,128]{2,0,1:T(8,128)S(1)})) conditional(s32[]{:T(128)} %convert_element_type.110, (f32[512,2,2,64]{0,3,2,1:T(8,128)S(1)}, f32[512,2,128]{2,0,1:T(8,128)S(1)}) %tuple.151, (s32[]{:T(128)}, s32[]{:T(128)}, s32[512]{0:T(512)S(1)}, bf16[4096,256]{0,1:T(8,128)(2,1)}, ...), branch_computations={%region_9.9_spmd, %region_10.10_spmd} | conditional | flops 547881984 | bytes 43118784 | solution.py:177
  171.6 3.2 %exponential_select_fusion = f32[2,2,512,512]{3,2,1,0:T(8,128)} fusion(bf16[512,2,2,64]{0,3,2,1:T(8,128)(2,1)S(1)} %bitcast.167, bf16[512,2,2,64]{0,3,2,1:T(8,128)(2,1)S(1)} %get-tuple-element.842, f32[2,2,512]{2,1,0:T(2,128)S(1)} %bitcast.180, pred[512,512]{1,0:T(8,128)(4,1)S(1)} %broadcast_compare_fusion.1), kind=kOutput, calls=%fused_computation.24 | convolution fusion | flops 137363456 | bytes 4988928 | tf_op jit(solution)/shard_map/while/body/eval_jaxpr/cond/branch_1_fun/qhcd,khcd->hcqk/dot_general | solution.py:41
  180.9 10.7 %conditional.8 = ((f32[512,2,2,64]{0,3,2,1:T(8,128)S(1)}, f32[512,2,128]{2,0,1:T(8,128)S(1)})) conditional(s32[]{:T(128)} %convert_element_type.110, (f32[512,2,2,64]{0,3,2,1:T(8,128)S(1)}, f32[512,2,128]{2,0,1:T(8,128)S(1)}) %tuple.151, (s32[]{:T(128)}, s32[]{:T(128)}, s32[512]{0:T(512)S(1)}, bf16[4096,256]{0,1:T(8,128)(2,1)}, ...), branch_computations={%region_9.9_spmd, %region_10.10_spmd} | conditional | flops 547881984 | bytes 43118784 | solution.py:177
  182.3 3.2 %exponential_select_fusion = f32[2,2,512,512]{3,2,1,0:T(8,128)} fusion(bf16[512,2,2,64]{0,3,2,1:T(8,128)(2,1)S(1)} %bitcast.167, bf16[512,2,2,64]{0,3,2,1:T(8,128)(2,1)S(1)} %get-tuple-element.842, f32[2,2,512]{2,1,0:T(2,128)S(1)} %bitcast.180, pred[512,512]{1,0:T(8,128)(4,1)S(1)} %broadcast_compare_fusion.1), kind=kOutput, calls=%fused_computation.24 | convolution fusion | flops 137363456 | bytes 4988928 | tf_op jit(solution)/shard_map/while/body/eval_jaxpr/cond/branch_1_fun/qhcd,khcd->hcqk/dot_general | solution.py:41
  191.7 10.7 %conditional.8 = ((f32[512,2,2,64]{0,3,2,1:T(8,128)S(1)}, f32[512,2,128]{2,0,1:T(8,128)S(1)})) conditional(s32[]{:T(128)} %convert_element_type.110, (f32[512,2,2,64]{0,3,2,1:T(8,128)S(1)}, f32[512,2,128]{2,0,1:T(8,128)S(1)}) %tuple.151, (s32[]{:T(128)}, s32[]{:T(128)}, s32[512]{0:T(512)S(1)}, bf16[4096,256]{0,1:T(8,128)(2,1)}, ...), branch_computations={%region_9.9_spmd, %region_10.10_spmd} | conditional | flops 547881984 | bytes 43118784 | solution.py:177
  202.4 3.9 %fusion.28 = f32[2048,256]{1,0:T(8,128)} fusion(bf16[512,4096]{1,0:T(8,128)(2,1)} %copy-done.10, s32[]{:T(128)S(6)} %select_n.52, f32[512,256]{1,0:T(8,128)S(1)} %copy_bitcast_fusion.2), kind=kOutput, calls=%fused_computation.46 | convolution fusion | flops 537001984 | bytes 4718596 | tf_op jit(solution)/shard_map/dot_general | solution.py:187
  208.4 8.3 %all-gather.7.cloned.1.call-done = bf16[4096,256]{0,1:T(8,128)(2,1)} async-done(((bf16[512,256]{0,1:T(8,128)(2,1)}), bf16[4096,256]{0,1:T(8,128)(2,1)}) %all-gather.7.cloned.1.call-update) | async-done | bytes 2097168 | tf_op jit(solution)/shard_map/all_gather | solution.py:90
  216.9 4.3 %while.38 = (s32[]{:T(128)}, f32[512,2,2,64]{0,3,2,1:T(8,128)S(1)}, s32[]{:T(128)}, bf16[4096,256]{0,1:T(8,128)(2,1)}, bf16[512,2,2,64]{0,3,2,1:T(8,128)(2,1)S(1...) while((s32[]{:T(128)}, f32[512,2,2,64]{0,3,2,1:T(8,128)S(1)}, ...), condition=%wide.region_7.8_spmd.clone, body=%wide.region_4.7_spmd.clone.sunk | while | flops 411960320 | bytes 20756812 | solution.py:125
  216.9 3.9 %conditional.7 = (f32[512,2,2,64]{0,3,2,1:T(8,128)S(1)}) conditional(s32[]{:T(128)} %convert_element_type.109, f32[512,2,2,64]{0,3,2,1:T(8,128)S(1)} %get-tuple-element.1241, (s32[]{:T(128)}, s32[512]{0:T(512)S(1)}, s32[]{:T(128)}, bf16[4096,256]{0,1:T(8,128)(2,1)}, bf16[512,2,2,64]{0,3,2,1:T(8,128)(2,1)S(1)}, /*index=5*/f32[512,2,2]{0,2,1:T(2,128)S(1)}, ...), branch_computations={%region_5.5_spmd, %region_6.6_spmd} | conditional | flops 411960320 | bytes 20754510 | solution.py:123
  222.2 65.1 %reduce-scatter.2.cloned.1.call-done = f32[256,256]{1,0:T(8,128)} async-done(((f32[2048,256]{1,0:T(8,128)}), f32[256,256]{1,0:T(8,128)}) %reduce-scatter.2.cloned.1.call-update) | async-done | bytes 262160 | tf_op jit(solution)/shard_map/reduce_scatter | solution.py:186
  (248 shorter events, 94.1 us)
Async XLA Ops:
  7.2 42.4 %copy-start = (bf16[2048,256]{1,0:T(8,128)(2,1)S(1)}, bf16[2048,256]{1,0:T(8,128)(2,1)}, u32[]{:S(2)}) copy-start(bf16[2048,256]{1,0:T(8,128)(2,1)} %param.20) | copy-start | bytes 3145732
  7.2 4.4 %copy-start.15 = (f32[128]{0:T(128)S(1)}, f32[128]{0:T(128)}, u32[]{:S(2)}) copy-start(f32[128]{0:T(128)} %param.25) | copy-start | bytes 1540
  7.2 4.4 %copy-start.12 = (f32[2]{0:T(128)S(1)}, f32[2]{0:T(128)}, u32[]{:S(2)}) copy-start(f32[2]{0:T(128)} %param.24) | copy-start | bytes 28
  7.2 109.0 %all-gather.9.cloned.1.call-start = ((), (), s32[]{:S(2)}) async-start(), calls=%async_computation.3 | async-start | bytes 2359296 | tf_op jit(solution)/shard_map/all_gather | solution.py:127
  9.1 107.1 %all-gather.11.cloned.1.call-start = ((), (), s32[]{:S(2)}) async-start(), calls=%async_computation.4 | async-start | bytes 2359296 | tf_op jit(solution)/shard_map/all_gather | solution.py:128
  13.1 195.3 %all-gather.5.cloned.1.call-start = ((), (), s32[]{:S(2)}) async-start(), calls=%async_computation.1 | async-start | bytes 2359296 | tf_op jit(solution)/shard_map/all_gather | solution.py:89
  15.0 201.8 %all-gather.7.cloned.1.call-start = ((), (), s32[]{:S(2)}) async-start(), calls=%async_computation.2 | async-start | bytes 2359296 | tf_op jit(solution)/shard_map/all_gather | solution.py:90
  15.0 9.4 %collective-permute-start = (bf16[512,512]{1,0:T(8,128)(2,1)S(1)}, bf16[512,512]{1,0:T(8,128)(2,1)S(1)}, u32[]{:S(2)}, u32[]{:S(2)}) collective-permute-start(bf16[512,512]{1,0:T(8,128)(2,1)S(1)} %copy-done.2), channel_id=1, source_target_pairs={{0,1},{1,2},{2,3},{3,0},{4,5},{5,6},{6,7},{7,4},{8,9},{9,10},{10,1... | collective-permute-start | bytes 1572872 | tf_op jit(solution)/shard_map/ppermute | solution.py:74
  25.2 8.7 %collective-permute-start.1 = (bf16[512,512]{1,0:T(8,128)(2,1)S(1)}, bf16[512,512]{1,0:T(8,128)(2,1)}, u32[]{:S(2)}, u32[]{:S(2)}) collective-permute-start(bf16[512,512]{1,0:T(8,128)(2,1)S(1)} %collective-permute-done), channel_id=1, source_target_pairs={{0,1},{1,2},{2,3},{3,0},{4,5},{5,6},{6,7},{7,4},{8,9},{9,10},{10,1... | collective-permute-start | bytes 1572872 | tf_op jit(solution)/shard_map/ppermute | solution.py:74
  33.9 8.9 %collective-permute-start.2 = (bf16[512,512]{1,0:T(8,128)(2,1)}, bf16[512,512]{1,0:T(8,128)(2,1)}, u32[]{:S(2)}, u32[]{:S(2)}) collective-permute-start(bf16[512,512]{1,0:T(8,128)(2,1)} %collective-permute-done.1), channel_id=1, source_target_pairs={{0,1},{1,2},{2,3},{3,0},{4,5},{5,6},{6,7},{7,4},{8,9},{9,10},{10,1... | collective-permute-start | bytes 1572872 | tf_op jit(solution)/shard_map/ppermute | solution.py:74
  33.9 11.2 %copy-start.4 = (bf16[512,512]{1,0:T(8,128)(2,1)S(1)}, bf16[512,512]{1,0:T(8,128)(2,1)}, u32[]{:S(2)}) copy-start(bf16[512,512]{1,0:T(8,128)(2,1)} %copy-done.3) | copy-start | bytes 1572868
  51.0 65.0 %copy-start.8 = (bf16[512,256]{0,1:T(8,128)(2,1)S(1)}, bf16[512,256]{0,1:T(8,128)(2,1)}, u32[]{:S(2)}) copy-start(bf16[512,256]{0,1:T(8,128)(2,1)} %fusion.32) | copy-start | bytes 786436
  51.0 65.3 %copy-start.7 = (bf16[512,256]{0,1:T(8,128)(2,1)S(1)}, bf16[512,256]{0,1:T(8,128)(2,1)}, u32[]{:S(2)}) copy-start(bf16[512,256]{0,1:T(8,128)(2,1)} %copy.46) | copy-start | bytes 786436
  51.1 236.2 %reduce-scatter.2.cloned.1.call-start = ((), (), s32[]{:S(2)}) async-start(), calls=%async_computation.5 | async-start | bytes 2359296 | tf_op jit(solution)/shard_map/reduce_scatter | solution.py:186
  117.8 3.3 %copy-start.13 = (f32[2]{0:T(128)S(1)}, f32[2]{0:T(128)}, u32[]{:S(2)}) copy-start(f32[2]{0:T(128)} %get-tuple-element.847) | copy-start | bytes 28 | tf_op jit(solution)/shard_map/while/body/eval_jaxpr/cond
  139.3 3.3 %copy-start.13 = (f32[2]{0:T(128)S(1)}, f32[2]{0:T(128)}, u32[]{:S(2)}) copy-start(f32[2]{0:T(128)} %get-tuple-element.847) | copy-start | bytes 28 | tf_op jit(solution)/shard_map/while/body/eval_jaxpr/cond
  150.2 3.3 %copy-start.13 = (f32[2]{0:T(128)S(1)}, f32[2]{0:T(128)}, u32[]{:S(2)}) copy-start(f32[2]{0:T(128)} %get-tuple-element.847) | copy-start | bytes 28 | tf_op jit(solution)/shard_map/while/body/eval_jaxpr/cond
  160.9 3.3 %copy-start.13 = (f32[2]{0:T(128)S(1)}, f32[2]{0:T(128)}, u32[]{:S(2)}) copy-start(f32[2]{0:T(128)} %get-tuple-element.847) | copy-start | bytes 28 | tf_op jit(solution)/shard_map/while/body/eval_jaxpr/cond
  171.6 3.3 %copy-start.13 = (f32[2]{0:T(128)S(1)}, f32[2]{0:T(128)}, u32[]{:S(2)}) copy-start(f32[2]{0:T(128)} %get-tuple-element.847) | copy-start | bytes 28 | tf_op jit(solution)/shard_map/while/body/eval_jaxpr/cond
  182.3 3.3 %copy-start.13 = (f32[2]{0:T(128)S(1)}, f32[2]{0:T(128)}, u32[]{:S(2)}) copy-start(f32[2]{0:T(128)} %get-tuple-element.847) | copy-start | bytes 28 | tf_op jit(solution)/shard_map/while/body/eval_jaxpr/cond
  193.0 3.3 %copy-start.13 = (f32[2]{0:T(128)S(1)}, f32[2]{0:T(128)}, u32[]{:S(2)}) copy-start(f32[2]{0:T(128)} %get-tuple-element.847) | copy-start | bytes 28 | tf_op jit(solution)/shard_map/while/body/eval_jaxpr/cond
  202.4 3.9 %copy-start.9 = (f32[512,256]{1,0:T(8,128)}, f32[512,256]{1,0:T(8,128)S(1)}, u32[]{:S(2)}) copy-start(f32[512,256]{1,0:T(8,128)S(1)} %copy_bitcast_fusion.2) | copy-start | bytes 1572868
  206.3 10.5 %copy-start.6 = (bf16[512,256]{0,1:T(8,128)(2,1)S(1)}, bf16[512,256]{0,1:T(8,128)(2,1)}, u32[]{:S(2)}) copy-start(bf16[512,256]{0,1:T(8,128)(2,1)} %copy.47) | copy-start | bytes 786436
  206.3 10.5 %copy-start.14 = (f32[2]{0:T(128)S(1)}, f32[2]{0:T(128)}, u32[]{:S(2)}) copy-start(f32[2]{0:T(128)} %get-tuple-element.1334) | copy-start | bytes 28
  (14 other events, 28.7 us)
Sparse Core Ops, SparseCore 0:
  10.1 53.2 all-gather.8
  66.0 48.9 all-gather.10
  117.6 48.6 all-gather.4
  168.2 48.5 all-gather.6
  220.7 66.5 reduce-scatter.1
